TPU v7x, 32 devices: a whole 2x2x4 slice. The times are simulated.
32 devices in a mesh: sp: 16 (over z, y, x), tp: 2 (over core).
Axes of the slice: x: 2, y: 2, z: 4, core: 2. Of those that a mesh axis runs over, the one named last changes fastest.
Arguments:
- residual: bfloat16 [3072, 2048], P(('sp', 'tp')), may hold values from -6 to 6
- queries_narrow: bfloat16 [3072, 512], P('sp', 'tp'), may hold values from -24 to 24
- keys_narrow: bfloat16 [3072, 512], P('sp', 'tp'), may hold values from -24 to 24
- values_narrow: bfloat16 [3072, 512], P('sp', 'tp'), may hold values from -6 to 6
- queries_broad: bfloat16 [3072, 512], P('sp', 'tp'), may hold values from -24 to 24
- keys_broad: bfloat16 [3072, 512], P('sp', 'tp'), may hold values from -24 to 24
- values_broad: bfloat16 [3072, 512], P('sp', 'tp'), may hold values from -6 to 6
- gates_narrow: float32 [3072, 16], P('sp', 'tp'), may hold values from -3072 to 0, as said below
- gates_broad: float32 [3072, 8], P('sp', 'tp'), may hold values from -3072 to 0, as said below
- project_narrow: bfloat16 [512, 2048], P('tp'), may hold values from -0.5 to 0.5
- project_broad: bfloat16 [512, 2048], P('tp'), may hold values from -0.5 to 0.5
- norm_gain: float32 [2048], replicated, may hold values from 0.1 to 1.9
- up_weight: bfloat16 [2048, 8192], P('sp', 'tp'), may hold values from -0.125 to 0.125
- down_weight: bfloat16 [8192, 2048], P('tp', 'sp'), may hold values from -0.0625 to 0.0625
Outputs:
- layer_out: bfloat16 [3072, 2048], P(('sp', 'tp'))
Inputs may be any that keep to these rules, and one draw needn't show every extreme that they name: `gates_narrow`: each head's cumulative log gate never rises from one position to the next. `gates_broad`: each head's cumulative log gate never rises from one position to the next.
All inputs are finite; a program needn't handle non-finite values.
Results may differ from a plain program's by a relative error of at most 0.018.
Values may be sent and summed in bfloat16 or wider, within the bound.
A program may use at most 128 MiB of HBM per device.

v0:
```python
import jax
import jax.numpy as jnp
from jax import lax
from jax.sharding import PartitionSpec as P

A_DIM = 32
B_DIM = 64


def group_update(state, queries, keys, values, query_gates, key_gates, allowed, head_size):
    peak, total, summed = state
    query_count = queries.shape[0]
    key_count = keys.shape[0]
    heads = queries.shape[1] // head_size
    scores = jnp.einsum(
        "qhd,khd->hqk",
        queries.reshape(query_count, heads, head_size),
        keys.reshape(key_count, heads, head_size),
        preferred_element_type=jnp.float32,
    ) * head_size ** (-0.5)
    scores = scores + query_gates.T[:, :, None] - key_gates.T[:, None, :]
    scores = jnp.where(allowed[None], scores, -1e30)
    new_peak = jnp.maximum(peak, jnp.max(scores, axis=-1))
    weights = jnp.exp(scores - new_peak[..., None]) * allowed[None].astype(jnp.float32)
    total = jnp.sum(weights, axis=-1)
    summed = jnp.einsum(
        "hqk,khd->hqd",
        weights.astype(jnp.bfloat16),
        values.reshape(key_count, heads, head_size),
        preferred_element_type=jnp.float32,
    )
    return (new_peak, total, summed)


def empty_state(query_count, heads, head_size):
    return (
        jnp.full((heads, query_count), -1e30, jnp.float32),
        jnp.zeros((heads, query_count), jnp.float32),
        jnp.zeros((heads, query_count, head_size), jnp.float32),
    )


def finish_group(state, head_size):
    peak, total, summed = state
    result = summed / total[..., None]
    return (
        result.transpose(1, 0, 2)
        .reshape(result.shape[1], result.shape[0] * head_size)
        .astype(jnp.bfloat16)
    )


def rms_scaled(mixed, norm_gain):
    mixed_wide = mixed.astype(jnp.float32)
    scale = lax.rsqrt(jnp.mean(mixed_wide * mixed_wide, axis=-1, keepdims=True) + 1e-06)
    return (mixed_wide * scale * norm_gain).astype(jnp.bfloat16)


def local(
    residual,
    queries_narrow,
    keys_narrow,
    values_narrow,
    queries_broad,
    keys_broad,
    values_broad,
    gates_narrow,
    gates_broad,
    project_narrow,
    project_broad,
    norm_gain,
    up_weight,
    down_weight,
):
    local_count = queries_narrow.shape[0]
    table_narrow, table_broad = (
        lax.all_gather(gates_narrow, "sp", axis=0, tiled=True),
        lax.all_gather(gates_broad, "sp", axis=0, tiled=True),
    )
    query_pos = lax.axis_index("sp") * local_count + jnp.arange(local_count, dtype=jnp.int32)
    initial = (
        empty_state(local_count, queries_narrow.shape[1] // A_DIM, A_DIM),
        empty_state(local_count, queries_broad.shape[1] // B_DIM, B_DIM),
    )
    piece_keys_narrow = lax.all_gather(keys_narrow, "sp", axis=0, tiled=True)
    piece_values_narrow = lax.all_gather(values_narrow, "sp", axis=0, tiled=True)
    piece_keys_broad = lax.all_gather(keys_broad, "sp", axis=0, tiled=True)
    piece_values_broad = lax.all_gather(values_broad, "sp", axis=0, tiled=True)
    piece_count = piece_keys_narrow.shape[0]
    key_pos = jnp.arange(piece_count, dtype=jnp.int32)
    allowed = key_pos[None, :] <= query_pos[:, None]
    state_narrow = group_update(
        initial[0],
        queries_narrow,
        piece_keys_narrow,
        piece_values_narrow,
        gates_narrow,
        table_narrow,
        allowed,
        A_DIM,
    )
    state_broad = group_update(
        initial[1],
        queries_broad,
        piece_keys_broad,
        piece_values_broad,
        gates_broad,
        table_broad,
        allowed,
        B_DIM,
    )
    attended_narrow = finish_group(state_narrow, A_DIM)
    attended_broad = finish_group(state_broad, B_DIM)
    projected = lax.psum_scatter(
        (
            jnp.dot(attended_narrow, project_narrow, preferred_element_type=jnp.float32)
            + jnp.dot(attended_broad, project_broad, preferred_element_type=jnp.float32)
        ).astype(jnp.bfloat16),
        "tp",
        scatter_dimension=0,
        tiled=True,
    ).astype(jnp.float32)
    mixed = (residual.astype(jnp.float32) + projected).astype(jnp.bfloat16)
    features = lax.all_gather(rms_scaled(mixed, norm_gain), "tp", axis=0, tiled=True)
    up_total = jnp.dot(
        features,
        lax.all_gather(up_weight, "sp", axis=0, tiled=True),
        preferred_element_type=jnp.float32,
    )
    hidden = jnp.square(jax.nn.relu(up_total)).astype(jnp.bfloat16)
    down_term = jnp.dot(
        hidden,
        lax.all_gather(down_weight, "sp", axis=1, tiled=True),
        preferred_element_type=jnp.float32,
    )
    summed_rows = lax.psum_scatter(
        down_term.astype(jnp.bfloat16), "tp", scatter_dimension=0, tiled=True
    ).astype(jnp.float32)
    return (mixed.astype(jnp.float32) + summed_rows).astype(jnp.bfloat16)


def solution(mesh):
    return jax.shard_map(
        local,
        mesh=mesh,
        in_specs=(
            P(("sp", "tp"), None),
            P("sp", "tp"),
            P("sp", "tp"),
            P("sp", "tp"),
            P("sp", "tp"),
            P("sp", "tp"),
            P("sp", "tp"),
            P("sp", "tp"),
            P("sp", "tp"),
            P("tp", None),
            P("tp", None),
            P(),
            P("sp", "tp"),
            P("tp", "sp"),
        ),
        out_specs=P(("sp", "tp"), None),
        check_vma=False,
    )
```

profile of v0, /device:TPU:0, one launch (start us, length us, event | category | flops | bytes accessed | tf_op | source)
XLA Modules:
  0.0 742.3 jit_solution(3498710460941625432)
XLA Ops:
  6.5 0.7 all-gather.9.cloned.1.call-update
  7.3 0.0 all-gather.13.cloned.1.call-start
  7.3 0.7 all-gather.13.cloned.1.call-update
  8.0 0.0 all-gather.11.cloned.1.call-start
  8.1 0.7 all-gather.11.cloned.1.call-update
  8.7 0.0 all-gather.15.cloned.1.call-start
  8.8 0.5 all-gather.15.cloned.1.call-update
  9.3 0.0 reduce-scatter.3.cloned.1.call-start
  9.4 1.3 iota_compare_fusion
  10.7 43.5 %all-gather = f32[16,192,8]{1,2,0:T(8,128)S(1)} all-gather(f32[1,192,8]{1,2,0:T(8,128)} %bitcast.59), channel_id=1, replica_groups=mesh['sp'=16,'tp'=2] {'sp'}, dimensions={0}, use_global_device_ids=true | all-gather | bytes 104448 | tf_op jit(solution)/shard_map/all_gather | solution.py:77
  54.3 0.7 reshape.92
  55.0 1.7 copy.29
  56.7 36.3 %all-gather.1 = f32[16,192,4]{1,2,0:T(4,128)S(1)} all-gather(f32[1,192,4]{1,2,0:T(4,128)} %bitcast.65), channel_id=1, replica_groups=mesh['sp'=16,'tp'=2] {'sp'}, dimensions={0}, use_global_device_ids=true | all-gather | bytes 52224 | tf_op jit(solution)/shard_map/all_gather | solution.py:78
  93.0 0.1 reshape.94
  93.1 1.6 copy.33
  94.7 2.6 copy.30
  97.3 7.4 fusion.2
  104.8 6.4 copy-done.4
  111.2 0.4 copy-done.14
  111.5 8.6 %fusion = f32[8,192]{1,0:T(8,128)} fusion(f32[8,192,3072]{2,1,0:T(8,128)S(1)} %get-tuple-element.8, f32[192,3072]{1,0:T(8,128)S(1)} %get-tuple-element.6, f32[8,192]{1,0:T(8,128)S(1)} %broadcast_maximum_fusion, f32[8,3072]{1,0:T(8,128)S(1)} %bitcast.53, f32[8,192]{1,0:T(8,128)S(1)} %bitcast.61, pred[192,3072]{1,0:T(8,128)(4,1)S(1)} %copy-done.8), kind=kLoop, calls=%fused_computation.2 | loop fusion | flops 33028608 | bytes 21940224 | tf_op jit(solution)/shard_map/reduce_sum | solution.py:25
  120.2 10.4 %all-gather.13.cloned.1.call-done = bf16[3072,256]{1,0:T(8,128)(2,1)} async-done(((bf16[192,256]{1,0:T(8,128)(2,1)}), bf16[3072,256]{1,0:T(8,128)(2,1)}) %all-gather.13.cloned.1.call-update) | async-done | bytes 1572880 | tf_op jit(solution)/shard_map/all_gather | solution.py:87
  130.6 2.6 copy.34
  133.2 8.0 %fusion.41 = (f32[4,192]{1,0:T(4,128)S(1)}, f32[4,192,3072]{2,1,0:T(8,128)}) fusion(f32[4,3072]{1,0:T(4,128)S(1)} %bitcast.58, f32[4,192]{1,0:T(4,128)} %bitcast.66, bf16[192,4,64]{0,2,1:T(8,128)(2,1)} %bitcast.55, bf16[3072,4,64]{0,2,1:T(8,128)(2,1)} %bitcast.49, pred[192,3072]{1,0:T(8,128)(4,1)} %get-tuple-element.5), kind=kOutput, calls=%fused_computation.43 | convolution fusion | flops 313785600 | bytes 11753472 | tf_op jit(solution)/shard_map/qhd,khd->hqk/dot_general | solution.py:15
  141.1 48.9 %all-gather.11.cloned.1.call-done = bf16[3072,256]{1,0:T(8,128)(2,1)} async-done(((bf16[192,256]{1,0:T(8,128)(2,1)}), bf16[3072,256]{1,0:T(8,128)(2,1)}) %all-gather.11.cloned.1.call-update) | async-done | bytes 1572880 | tf_op jit(solution)/shard_map/all_gather | solution.py:86
  190.1 2.7 copy.32
  192.8 11.0 %fusion.24 = bf16[192,8,32]{0,2,1:T(8,128)(2,1)S(1)} fusion(bf16[3072,8,32]{0,2,1:T(8,128)(2,1)} %bitcast.48, f32[8,192,3072]{2,1,0:T(8,128)} %copy-done.4, f32[192,3072]{1,0:T(8,128)} %copy-done.2, f32[8,192]{1,0:T(8,128)S(1)} %copy-done.15, f32[8,3072]{1,0:T(8,128)S(1)} %bitcast.54, f32[8,192]{1,0:T(8,128)S(1)} %bitcast.62, ...), kind=kOutput, calls=%fused_computation.27 | convolution fusion | flops 335118336 | bytes 23611392 | tf_op jit(solution)/shard_map/hqk,khd->hqd/dot_general | solution.py:26
  203.8 1.6 fusion.42
  205.4 1.8 fusion.6
  207.3 42.1 %all-gather.15.cloned.1.call-done = bf16[3072,256]{1,0:T(8,128)(2,1)} async-done(((bf16[192,256]{1,0:T(8,128)(2,1)}), bf16[3072,256]{1,0:T(8,128)(2,1)}) %all-gather.15.cloned.1.call-update) | async-done | bytes 1572880 | tf_op jit(solution)/shard_map/all_gather | solution.py:88
  249.4 2.6 copy.36
  252.0 6.7 fusion.30
  258.8 1.3 fusion.14
  260.1 0.0 reduce-scatter.3.cloned.1.call-update
  260.1 0.0 all-gather.17.cloned.1.call-start
  260.2 0.5 all-gather.17.cloned.1.call-update
  260.7 0.0 all-gather.19.cloned.1.call-start
  260.7 0.7 all-gather.19.cloned.1.call-update
  261.4 0.0 reduce-scatter.5.cloned.1.call-start
  261.5 5.7 reduce-scatter.3.cloned.1.call-done
  267.1 1.2 fusion.33
  268.4 1.2 fusion.35
  269.6 2.4 all_gather.33
  271.9 190.0 %all-gather.17.cloned.1.call-done = bf16[2048,4096]{1,0:T(8,128)(2,1)} async-done(((bf16[128,4096]{1,0:T(8,128)(2,1)}), bf16[2048,4096]{1,0:T(8,128)(2,1)}) %all-gather.17.cloned.1.call-update) | async-done | bytes 16777232 | tf_op jit(solution)/shard_map/all_gather | solution.py:127
  461.9 250.0 %all-gather.19.cloned.1.call-done = bf16[4096,2048]{1,0:T(8,128)(2,1)} async-done(((bf16[4096,128]{1,0:T(8,128)(2,1)}), bf16[4096,2048]{1,0:T(8,128)(2,1)}) %all-gather.19.cloned.1.call-update) | async-done | bytes 16777232 | tf_op jit(solution)/shard_map/all_gather | solution.py:133
  711.9 15.1 %convolution_convert_fusion = bf16[192,2048]{1,0:T(8,128)(2,1)} fusion(bf16[4096,2048]{1,0:T(8,128)(2,1)} %all-gather.19.cloned.1.call-done, bf16[192,2048]{1,0:T(8,128)(2,1)S(1)} %all_gather.33, bf16[2048,4096]{1,0:T(8,128)(2,1)} %all-gather.17.cloned.1.call-done), kind=kOutput, calls=%fused_computation.18 | convolution fusion | flops 6445203456 | bytes 35127296 | tf_op jit(solution)/shard_map/dot_general | solution.py:131
  727.0 0.0 reduce-scatter.5.cloned.1.call-update
  727.0 6.5 reduce-scatter.5.cloned.1.call-done
  733.5 1.9 fusion.36
  (49 shorter events, 0.2 us)
Async XLA Ops:
  6.5 197.3 %copy-start = (bf16[256,2048]{1,0:T(8,128)(2,1)S(1)}, bf16[256,2048]{1,0:T(8,128)(2,1)}, u32[]{:S(2)}) copy-start(bf16[256,2048]{1,0:T(8,128)(2,1)} %param.23) | copy-start | bytes 3145732
  6.5 88.2 %all-gather.9.cloned.1.call-start = ((), (), s32[]{:S(2)}) async-start(), calls=%async_computation.2 | async-start | bytes 1671168 | tf_op jit(solution)/shard_map/all_gather | solution.py:85
  7.3 123.3 %all-gather.13.cloned.1.call-start = ((), (), s32[]{:S(2)}) async-start(), calls=%async_computation.4 | async-start | bytes 1671168 | tf_op jit(solution)/shard_map/all_gather | solution.py:87
  8.0 182.0 %all-gather.11.cloned.1.call-start = ((), (), s32[]{:S(2)}) async-start(), calls=%async_computation.3 | async-start | bytes 1671168 | tf_op jit(solution)/shard_map/all_gather | solution.py:86
  8.7 240.7 %all-gather.15.cloned.1.call-start = ((), (), s32[]{:S(2)}) async-start(), calls=%async_computation.5 | async-start | bytes 1671168 | tf_op jit(solution)/shard_map/all_gather | solution.py:88
  9.3 257.8 %reduce-scatter.3.cloned.1.call-start = ((), (), s32[]{:S(2)}) async-start(), calls=%async_computation.6 | async-start | bytes 1179648 | tf_op jit(solution)/shard_map/reduce_scatter | solution.py:114
  10.7 94.0 %copy-start.2 = (f32[192,3072]{1,0:T(8,128)}, f32[192,3072]{1,0:T(8,128)S(1)}, u32[]{:S(2)}) copy-start(f32[192,3072]{1,0:T(8,128)S(1)} %get-tuple-element.6) | copy-start | bytes 7077892
  97.3 14.2 %copy-start.8 = (pred[192,3072]{1,0:T(8,128)(4,1)S(1)}, pred[192,3072]{1,0:T(8,128)(4,1)}, u32[]{:S(2)}) copy-start(pred[192,3072]{1,0:T(8,128)(4,1)} %get-tuple-element.5) | copy-start | bytes 1769476
  97.3 14.2 %copy-start.11 = (f32[3072,8]{0,1:T(8,128)S(1)}, f32[3072,8]{0,1:T(8,128)}, u32[]{:S(2)}) copy-start(f32[3072,8]{0,1:T(8,128)} %reshape.92) | copy-start | bytes 294916
  97.3 14.2 %copy-start.12 = (f32[192,8]{0,1:T(8,128)S(1)}, f32[192,8]{0,1:T(8,128)}, u32[]{:S(2)}) copy-start(f32[192,8]{0,1:T(8,128)} %param.21) | copy-start | bytes 18436
  104.7 6.4 copy-start.4
  104.7 6.8 copy-start.14
  133.2 59.6 %copy-start.9 = (pred[192,3072]{1,0:T(8,128)(4,1)S(1)}, pred[192,3072]{1,0:T(8,128)(4,1)}, u32[]{:S(2)}) copy-start(pred[192,3072]{1,0:T(8,128)(4,1)} %get-tuple-element.5) | copy-start | bytes 1769476
  133.2 59.6 %copy-start.13 = (f32[192,8]{0,1:T(8,128)S(1)}, f32[192,8]{0,1:T(8,128)}, u32[]{:S(2)}) copy-start(f32[192,8]{0,1:T(8,128)} %param.21) | copy-start | bytes 18436
  133.2 59.6 %copy-start.15 = (f32[8,192]{1,0:T(8,128)S(1)}, f32[8,192]{1,0:T(8,128)}, u32[]{:S(2)}) copy-start(f32[8,192]{1,0:T(8,128)} %copy-done.14) | copy-start | bytes 18436
  133.2 59.6 %copy-start.17 = (f32[8,192]{1,0:T(8,128)S(1)}, f32[8,192]{1,0:T(8,128)}, u32[]{:S(2)}) copy-start(f32[8,192]{1,0:T(8,128)} %fusion) | copy-start | bytes 18436
  190.0 15.4 %slice-start = ((s8[9437184]{0:T(1024)(128)(4,1)}), s8[1048576]{0:T(1024)(128)(4,1)S(1)}, s32[]{:S(2)}) async-start(s8[9437184]{0:T(1024)(128)(4,1)} %bitcast.45), calls=%async_computation.10 | async-start | bytes 2097152
  192.8 12.6 %slice-start.1 = ((s8[9437184]{0:T(1024)(128)(4,1)}), s8[4194304]{0:T(1024)(128)(4,1)S(1)}, s32[]{:S(2)}) async-start(s8[9437184]{0:T(1024)(128)(4,1)} %bitcast.45), calls=%async_computation.11 | async-start | bytes 8388608
  192.8 12.6 %slice-start.2 = ((s8[9437184]{0:T(1024)(128)(4,1)}), s8[4194304]{0:T(1024)(128)(4,1)S(1)}, s32[]{:S(2)}) async-start(s8[9437184]{0:T(1024)(128)(4,1)} %bitcast.45), calls=%async_computation.12 | async-start | bytes 8388608
  192.8 12.6 %copy-start.3 = (f32[192,3072]{1,0:T(8,128)S(1)}, f32[192,3072]{1,0:T(8,128)}, u32[]{:S(2)}) copy-start(f32[192,3072]{1,0:T(8,128)} %copy-done.2) | copy-start | bytes 7077892
  207.3 51.5 %copy-start.5 = (f32[192,2048]{1,0:T(8,128)S(1)}, f32[192,2048]{1,0:T(8,128)}, u32[]{:S(2)}) copy-start(f32[192,2048]{1,0:T(8,128)} %fusion.42) | copy-start | bytes 4718596
  207.3 51.5 %copy-start.10 = (bf16[256,2048]{1,0:T(8,128)(2,1)S(1)}, bf16[256,2048]{1,0:T(8,128)(2,1)}, u32[]{:S(2)}) copy-start(bf16[256,2048]{1,0:T(8,128)(2,1)} %param.24) | copy-start | bytes 3145732
  252.0 15.1 %copy-start.6 = (bf16[96,2048]{1,0:T(8,128)(2,1)S(1)}, bf16[96,2048]{1,0:T(8,128)(2,1)}, u32[]{:S(2)}) copy-start(bf16[96,2048]{1,0:T(8,128)(2,1)} %param.14) | copy-start | bytes 1179652
  252.0 16.4 %copy-start.16 = (f32[2048]{0:T(1024)S(1)}, f32[2048]{0:T(1024)}, u32[]{:S(2)}) copy-start(f32[2048]{0:T(1024)} %param.25) | copy-start | bytes 24580
  260.1 201.8 %all-gather.17.cloned.1.call-start = ((), (), s32[]{:S(2)}) async-start(), calls=%async_computation.7 | async-start | bytes 17825792 | tf_op jit(solution)/shard_map/all_gather | solution.py:127
  260.7 451.2 %all-gather.19.cloned.1.call-start = ((), (), s32[]{:S(2)}) async-start(), calls=%async_computation.8 | async-start | bytes 17825792 | tf_op jit(solution)/shard_map/all_gather | solution.py:133
  261.4 472.1 %reduce-scatter.5.cloned.1.call-start = ((), (), s32[]{:S(2)}) async-start(), calls=%async_computation.9 | async-start | bytes 1179648 | tf_op jit(solution)/shard_map/reduce_scatter | solution.py:136
  271.9 461.6 %copy-start.7 = (bf16[96,2048]{1,0:T(8,128)(2,1)S(1)}, bf16[96,2048]{1,0:T(8,128)(2,1)}, u32[]{:S(2)}) copy-start(bf16[96,2048]{1,0:T(8,128)(2,1)} %reduce-scatter.3.cloned.1.call-done) | copy-start | bytes 1179652
  711.9 23.5 %copy-start.1 = (bf16[256,2048]{1,0:T(8,128)(2,1)S(1)}, bf16[256,2048]{1,0:T(8,128)(2,1)}, u32[]{:S(2)}) copy-start(bf16[256,2048]{1,0:T(8,128)(2,1)} %param.23) | copy-start | bytes 3145732
Sparse Core Ops, SparseCore 0:
  10.1 60.9 all-gather.8
  73.8 56.6 all-gather.12
  133.3 56.6 all-gather.10
  192.7 56.7 all-gather.14
  260.2 6.8 reduce-scatter.2
  269.8 192.1 all-gather.16
  464.6 247.2 all-gather.18
  727.2 6.3 reduce-scatter.4
where the time goes:
time: 743 us; the launch traced here: 742 us
  waiting for transfers between devices  557 us (75%)
  blocking collectives  82.2 us (11%)
  matrix products  51.1 us (7%)
  local copies, waits for them, and re-layouts  21.5 us (3%)
  other arithmetic  16.1 us (2%)
  between operations  13.7 us (2%)
    all_gather x1, waiting for transfers between devices, local(): lax.all_gather(down_weight, 'sp', axis=1, tiled=True)  250 us
    all_gather x1, waiting for transfers between devices, local(): lax.all_gather(up_weight, 'sp', axis=0, tiled=True)  190 us
    all_gather x1, waiting for transfers between devices, local(): lax.all_gather(values_narrow, 'sp', axis=0, tiled=True)  48.9 us
    all_gather x1, blocking collectives, local(): lax.all_gather(gates_narrow, 'sp', axis=0, tiled=True)  43.5 us
    all_gather x1, waiting for transfers between devices, local(): piece_values_broad = lax.all_gather(values_broad, 'sp', axis=0, tiled=True)  42.1 us
    all_gather x1, blocking collectives, local(): lax.all_gather(gates_broad, 'sp', axis=0, tiled=True)  36.3 us
    dot_general x2, matrix products, group_update(): jnp.einsum('hqk,khd->hqd', weights.astype(jnp.bfloat16), values.reshape(k...  17.7 us
    dot_general x2, matrix products, group_update(): jnp.einsum('qhd,khd->hqk', queries.reshape(query_count, heads, head_size)...  15.4 us
  transfers between devices with their start and end apart: 8, of which 7 were waited for; matrix products, arithmetic and copies ran while one was open for 7% of the time, Pallas kernels for 0%

commit v1 on v0

--- a/solution.py
+++ b/solution.py
@@ -130,7 +130,7 @@
     hidden = jnp.square(jax.nn.relu(up_total)).astype(jnp.bfloat16)
     down_term = jnp.dot(
         hidden,
-        lax.all_gather(down_weight, "sp", axis=1, tiled=True),
+        jnp.concatenate(lax.all_gather(down_weight, "sp"), axis=1),
         preferred_element_type=jnp.float32,
     )
     summed_rows = lax.psum_scatter(

time: 743 us -> 686 us (0.923)
  waiting for transfers between devices: 557 us -> 478 us
  local copies, waits for them, and re-layouts: 21.5 us -> 42.8 us
    all_gather x1, waiting for transfers between devices: 250 us -> 190 us  [local(): lax.all_gather(down_weight, 'sp')]
    reshape x0 -> x1, local copies, waits for them, and re-layouts: none -> 21.3 us  [local(): jnp.concatenate(lax.all_gather(down_weight, 'sp'), axis=1)]
    all_gather x1, waiting for transfers between devices: 190 us -> 171 us  [local(): lax.all_gather(up_weight, 'sp', axis=0, tiled=True)]
  transfers between devices with their start and end apart: 8 -> 8, of which waited for: 7 -> 7; matrix products, arithmetic and copies ran while one was open for 7% -> 11% of each run, Pallas kernels for 0% -> 0%
where the time goes in v1:
time: 686 us; the launch traced here: 685 us
  waiting for transfers between devices  478 us (70%)
  blocking collectives  82.2 us (12%)
  matrix products  52.2 us (8%)
  local copies, waits for them, and re-layouts  42.8 us (6%)
  other arithmetic  16.1 us (2%)
  between operations  13.7 us (2%)
    all_gather x1, waiting for transfers between devices, local(): lax.all_gather(down_weight, 'sp')  190 us
    all_gather x1, waiting for transfers between devices, local(): lax.all_gather(up_weight, 'sp', axis=0, tiled=True)  171 us
    all_gather x1, waiting for transfers between devices, local(): lax.all_gather(values_narrow, 'sp', axis=0, tiled=True)  48.9 us
    all_gather x1, blocking collectives, local(): lax.all_gather(gates_narrow, 'sp', axis=0, tiled=True)  43.5 us
    all_gather x1, waiting for transfers between devices, local(): piece_values_broad = lax.all_gather(values_broad, 'sp', axis=0, tiled=True)  42.1 us
    all_gather x1, blocking collectives, local(): lax.all_gather(gates_broad, 'sp', axis=0, tiled=True)  36.3 us
    reshape x1, local copies, waits for them, and re-layouts, local(): jnp.concatenate(lax.all_gather(down_weight, 'sp'), axis=1)  21.3 us
    dot_general x2, matrix products, group_update(): jnp.einsum('hqk,khd->hqd', weights.astype(jnp.bfloat16), values.reshape(k...  17.7 us
  transfers between devices with their start and end apart: 8, of which 7 were waited for; matrix products, arithmetic and copies ran while one was open for 11% of the time, Pallas kernels for 0%

profile of v1, /device:TPU:0, one launch (start us, length us, event | category | flops | bytes accessed | tf_op | source)
XLA Modules:
  0.0 685.4 jit_solution(3921579949885772902)
XLA Ops:
  6.5 0.7 all-gather.10.cloned.1.call-update
  7.3 0.0 all-gather.14.cloned.1.call-start
  7.3 0.7 all-gather.14.cloned.1.call-update
  8.0 0.0 all-gather.12.cloned.1.call-start
  8.1 0.7 all-gather.12.cloned.1.call-update
  8.7 0.0 all-gather.16.cloned.1.call-start
  8.8 0.5 all-gather.16.cloned.1.call-update
  9.3 0.0 reduce-scatter.3.cloned.1.call-start
  9.4 1.3 iota_compare_fusion
  10.7 43.5 %all-gather.1 = f32[16,192,8]{1,2,0:T(8,128)S(1)} all-gather(f32[1,192,8]{1,2,0:T(8,128)} %bitcast.65), channel_id=1, replica_groups=mesh['sp'=16,'tp'=2] {'sp'}, dimensions={0}, use_global_device_ids=true | all-gather | bytes 104448 | tf_op jit(solution)/shard_map/all_gather | solution.py:77
  54.3 0.7 reshape.101
  55.0 1.7 copy.38
  56.7 36.3 %all-gather.2 = f32[16,192,4]{1,2,0:T(4,128)S(1)} all-gather(f32[1,192,4]{1,2,0:T(4,128)} %bitcast.71), channel_id=1, replica_groups=mesh['sp'=16,'tp'=2] {'sp'}, dimensions={0}, use_global_device_ids=true | all-gather | bytes 52224 | tf_op jit(solution)/shard_map/all_gather | solution.py:78
  93.0 0.1 reshape.103
  93.1 1.6 copy.42
  94.7 2.6 copy.39
  97.3 7.4 %fusion.2 = (f32[8,192]{1,0:T(8,128)S(1)}, f32[8,192,3072]{2,1,0:T(8,128)S(1)}) fusion(f32[8,3072]{1,0:T(8,128)} %bitcast.58, f32[8,192]{1,0:T(8,128)} %bitcast.66, pred[192,3072]{1,0:T(8,128)(4,1)} %get-tuple-element.5, bf16[192,8,32]{0,2,1:T(8,128)(2,1)} %bitcast.62, bf16[3072,8,32]{0,2,1:T(8,128)(2,1)} %bitcast.56), kind=kOutput, calls=%fused_computation.4 | convolution fusion | flops 325581312 | bytes 21245952 | tf_op jit(solution)/shard_map/qhd,khd->hqk/dot_general | solution.py:15
  104.8 6.4 copy-done.4
  111.2 0.4 copy-done.14
  111.5 8.6 %fusion = f32[8,192]{1,0:T(8,128)} fusion(f32[8,192,3072]{2,1,0:T(8,128)S(1)} %get-tuple-element.8, f32[192,3072]{1,0:T(8,128)S(1)} %get-tuple-element.6, f32[8,192]{1,0:T(8,128)S(1)} %broadcast_maximum_fusion, f32[8,3072]{1,0:T(8,128)S(1)} %bitcast.59, f32[8,192]{1,0:T(8,128)S(1)} %bitcast.67, pred[192,3072]{1,0:T(8,128)(4,1)S(1)} %copy-done.8), kind=kLoop, calls=%fused_computation.2 | loop fusion | flops 33028608 | bytes 21940224 | tf_op jit(solution)/shard_map/reduce_sum | solution.py:25
  120.2 10.4 %all-gather.14.cloned.1.call-done = bf16[3072,256]{1,0:T(8,128)(2,1)} async-done(((bf16[192,256]{1,0:T(8,128)(2,1)}), bf16[3072,256]{1,0:T(8,128)(2,1)}) %all-gather.14.cloned.1.call-update) | async-done | bytes 1572880 | tf_op jit(solution)/shard_map/all_gather | solution.py:87
  130.6 2.6 copy.43
  133.2 8.0 %fusion.41 = (f32[4,192]{1,0:T(4,128)S(1)}, f32[4,192,3072]{2,1,0:T(8,128)}) fusion(f32[4,3072]{1,0:T(4,128)S(1)} %bitcast.64, f32[4,192]{1,0:T(4,128)} %bitcast.72, bf16[192,4,64]{0,2,1:T(8,128)(2,1)} %bitcast.61, bf16[3072,4,64]{0,2,1:T(8,128)(2,1)} %bitcast.55, pred[192,3072]{1,0:T(8,128)(4,1)} %get-tuple-element.5), kind=kOutput, calls=%fused_computation.43 | convolution fusion | flops 313785600 | bytes 11753472 | tf_op jit(solution)/shard_map/qhd,khd->hqk/dot_general | solution.py:15
  141.1 48.9 %all-gather.12.cloned.1.call-done = bf16[3072,256]{1,0:T(8,128)(2,1)} async-done(((bf16[192,256]{1,0:T(8,128)(2,1)}), bf16[3072,256]{1,0:T(8,128)(2,1)}) %all-gather.12.cloned.1.call-update) | async-done | bytes 1572880 | tf_op jit(solution)/shard_map/all_gather | solution.py:86
  190.1 2.7 copy.41
  192.8 11.0 %fusion.24 = bf16[192,8,32]{0,2,1:T(8,128)(2,1)S(1)} fusion(bf16[3072,8,32]{0,2,1:T(8,128)(2,1)} %bitcast.54, f32[8,192,3072]{2,1,0:T(8,128)} %copy-done.4, f32[192,3072]{1,0:T(8,128)} %copy-done.2, f32[8,192]{1,0:T(8,128)S(1)} %copy-done.15, f32[8,3072]{1,0:T(8,128)S(1)} %bitcast.60, f32[8,192]{1,0:T(8,128)S(1)} %bitcast.68, ...), kind=kOutput, calls=%fused_computation.27 | convolution fusion | flops 335118336 | bytes 23611392 | tf_op jit(solution)/shard_map/hqk,khd->hqd/dot_general | solution.py:26
  203.8 1.6 fusion.42
  205.4 1.8 fusion.6
  207.3 42.1 %all-gather.16.cloned.1.call-done = bf16[3072,256]{1,0:T(8,128)(2,1)} async-done(((bf16[192,256]{1,0:T(8,128)(2,1)}), bf16[3072,256]{1,0:T(8,128)(2,1)}) %all-gather.16.cloned.1.call-update) | async-done | bytes 1572880 | tf_op jit(solution)/shard_map/all_gather | solution.py:88
  249.4 2.6 copy.45
  252.0 6.7 fusion.30
  258.8 1.3 fusion.14
  260.1 0.0 reduce-scatter.3.cloned.1.call-update
  260.1 0.0 all-gather.20.cloned.1.call-start
  260.2 0.5 all-gather.20.cloned.1.call-update
  260.7 0.0 all-gather.18.cloned.1.call-start
  260.7 0.7 all-gather.18.cloned.1.call-update
  261.4 0.0 reduce-scatter.5.cloned.1.call-start
  261.5 5.7 reduce-scatter.3.cloned.1.call-done
  267.1 1.2 fusion.33
  268.4 1.2 fusion.35
  269.6 2.4 all_gather.36
  271.9 190.0 %all-gather.20.cloned.1.call-done = bf16[65536,128]{1,0:T(8,128)(2,1)} async-done(((bf16[4096,128]{1,0:T(8,128)(2,1)}), bf16[65536,128]{1,0:T(8,128)(2,1)}) %all-gather.20.cloned.1.call-update) | async-done | bytes 16777232 | tf_op jit(solution)/shard_map/all_gather | solution.py:133
  461.9 21.3 %copy.46 = bf16[4096,16,128]{0,2,1:T(8,128)(2,1)} copy(bf16[4096,16,128]{2,0,1:T(8,128)(2,1)} %bitcast.51) | data formatting | bytes 33554432 | tf_op jit(solution)/shard_map/reshape | solution.py:133
  483.2 170.7 %all-gather.18.cloned.1.call-done = bf16[2048,4096]{1,0:T(8,128)(2,1)} async-done(((bf16[128,4096]{1,0:T(8,128)(2,1)}), bf16[2048,4096]{1,0:T(8,128)(2,1)}) %all-gather.18.cloned.1.call-update) | async-done | bytes 16777232 | tf_op jit(solution)/shard_map/all_gather | solution.py:127
  653.9 16.2 %convolution_convert_fusion = bf16[192,2048]{1,0:T(8,128)(2,1)} fusion(bf16[4096,2048]{0,1:T(8,128)(2,1)} %bitcast.52, bf16[192,2048]{1,0:T(8,128)(2,1)S(1)} %all_gather.36, bf16[2048,4096]{1,0:T(8,128)(2,1)} %all-gather.18.cloned.1.call-done), kind=kOutput, calls=%fused_computation.18 | convolution fusion | flops 6445203456 | bytes 35127296 | tf_op jit(solution)/shard_map/dot_general | solution.py:131
  670.1 6.5 reduce-scatter.5.cloned.1.call-done
  676.6 1.9 fusion.36
  (50 shorter events, 0.2 us)
Async XLA Ops:
  6.5 197.3 %copy-start = (bf16[256,2048]{1,0:T(8,128)(2,1)S(1)}, bf16[256,2048]{1,0:T(8,128)(2,1)}, u32[]{:S(2)}) copy-start(bf16[256,2048]{1,0:T(8,128)(2,1)} %param.23) | copy-start | bytes 3145732
  6.5 88.2 %all-gather.10.cloned.1.call-start = ((), (), s32[]{:S(2)}) async-start(), calls=%async_computation.2 | async-start | bytes 1671168 | tf_op jit(solution)/shard_map/all_gather | solution.py:85
  7.3 123.3 %all-gather.14.cloned.1.call-start = ((), (), s32[]{:S(2)}) async-start(), calls=%async_computation.4 | async-start | bytes 1671168 | tf_op jit(solution)/shard_map/all_gather | solution.py:87
  8.0 182.0 %all-gather.12.cloned.1.call-start = ((), (), s32[]{:S(2)}) async-start(), calls=%async_computation.3 | async-start | bytes 1671168 | tf_op jit(solution)/shard_map/all_gather | solution.py:86
  8.7 240.7 %all-gather.16.cloned.1.call-start = ((), (), s32[]{:S(2)}) async-start(), calls=%async_computation.5 | async-start | bytes 1671168 | tf_op jit(solution)/shard_map/all_gather | solution.py:88
  9.3 257.8 %reduce-scatter.3.cloned.1.call-start = ((), (), s32[]{:S(2)}) async-start(), calls=%async_computation.6 | async-start | bytes 1179648 | tf_op jit(solution)/shard_map/reduce_scatter | solution.py:114
  10.7 94.0 %copy-start.2 = (f32[192,3072]{1,0:T(8,128)}, f32[192,3072]{1,0:T(8,128)S(1)}, u32[]{:S(2)}) copy-start(f32[192,3072]{1,0:T(8,128)S(1)} %get-tuple-element.6) | copy-start | bytes 7077892
  97.3 14.2 %copy-start.8 = (pred[192,3072]{1,0:T(8,128)(4,1)S(1)}, pred[192,3072]{1,0:T(8,128)(4,1)}, u32[]{:S(2)}) copy-start(pred[192,3072]{1,0:T(8,128)(4,1)} %get-tuple-element.5) | copy-start | bytes 1769476
  97.3 14.2 %copy-start.11 = (f32[3072,8]{0,1:T(8,128)S(1)}, f32[3072,8]{0,1:T(8,128)}, u32[]{:S(2)}) copy-start(f32[3072,8]{0,1:T(8,128)} %reshape.101) | copy-start | bytes 294916
  97.3 14.2 %copy-start.12 = (f32[192,8]{0,1:T(8,128)S(1)}, f32[192,8]{0,1:T(8,128)}, u32[]{:S(2)}) copy-start(f32[192,8]{0,1:T(8,128)} %param.21) | copy-start | bytes 18436
  104.7 6.4 copy-start.4
  104.7 6.8 copy-start.14
  133.2 59.6 %copy-start.9 = (pred[192,3072]{1,0:T(8,128)(4,1)S(1)}, pred[192,3072]{1,0:T(8,128)(4,1)}, u32[]{:S(2)}) copy-start(pred[192,3072]{1,0:T(8,128)(4,1)} %get-tuple-element.5) | copy-start | bytes 1769476
  133.2 59.6 %copy-start.13 = (f32[192,8]{0,1:T(8,128)S(1)}, f32[192,8]{0,1:T(8,128)}, u32[]{:S(2)}) copy-start(f32[192,8]{0,1:T(8,128)} %param.21) | copy-start | bytes 18436
  133.2 59.6 %copy-start.15 = (f32[8,192]{1,0:T(8,128)S(1)}, f32[8,192]{1,0:T(8,128)}, u32[]{:S(2)}) copy-start(f32[8,192]{1,0:T(8,128)} %copy-done.14) | copy-start | bytes 18436
  133.2 59.6 %copy-start.17 = (f32[8,192]{1,0:T(8,128)S(1)}, f32[8,192]{1,0:T(8,128)}, u32[]{:S(2)}) copy-start(f32[8,192]{1,0:T(8,128)} %fusion) | copy-start | bytes 18436
  190.0 15.4 %slice-start = ((s8[9437184]{0:T(1024)(128)(4,1)}), s8[1048576]{0:T(1024)(128)(4,1)S(1)}, s32[]{:S(2)}) async-start(s8[9437184]{0:T(1024)(128)(4,1)} %bitcast.49), calls=%async_computation.10 | async-start | bytes 2097152
  192.8 12.6 %slice-start.1 = ((s8[9437184]{0:T(1024)(128)(4,1)}), s8[4194304]{0:T(1024)(128)(4,1)S(1)}, s32[]{:S(2)}) async-start(s8[9437184]{0:T(1024)(128)(4,1)} %bitcast.49), calls=%async_computation.11 | async-start | bytes 8388608
  192.8 12.6 %slice-start.2 = ((s8[9437184]{0:T(1024)(128)(4,1)}), s8[4194304]{0:T(1024)(128)(4,1)S(1)}, s32[]{:S(2)}) async-start(s8[9437184]{0:T(1024)(128)(4,1)} %bitcast.49), calls=%async_computation.12 | async-start | bytes 8388608
  192.8 12.6 %copy-start.3 = (f32[192,3072]{1,0:T(8,128)S(1)}, f32[192,3072]{1,0:T(8,128)}, u32[]{:S(2)}) copy-start(f32[192,3072]{1,0:T(8,128)} %copy-done.2) | copy-start | bytes 7077892
  207.3 51.5 %copy-start.5 = (f32[192,2048]{1,0:T(8,128)S(1)}, f32[192,2048]{1,0:T(8,128)}, u32[]{:S(2)}) copy-start(f32[192,2048]{1,0:T(8,128)} %fusion.42) | copy-start | bytes 4718596
  207.3 51.5 %copy-start.10 = (bf16[256,2048]{1,0:T(8,128)(2,1)S(1)}, bf16[256,2048]{1,0:T(8,128)(2,1)}, u32[]{:S(2)}) copy-start(bf16[256,2048]{1,0:T(8,128)(2,1)} %param.24) | copy-start | bytes 3145732
  252.0 15.1 %copy-start.6 = (bf16[96,2048]{1,0:T(8,128)(2,1)S(1)}, bf16[96,2048]{1,0:T(8,128)(2,1)}, u32[]{:S(2)}) copy-start(bf16[96,2048]{1,0:T(8,128)(2,1)} %param.14) | copy-start | bytes 1179652
  252.0 16.4 %copy-start.16 = (f32[2048]{0:T(1024)S(1)}, f32[2048]{0:T(1024)}, u32[]{:S(2)}) copy-start(f32[2048]{0:T(1024)} %param.25) | copy-start | bytes 24580
  260.1 201.8 %all-gather.20.cloned.1.call-start = ((), (), s32[]{:S(2)}) async-start(), calls=%async_computation.9 | async-start | bytes 17825792 | tf_op jit(solution)/shard_map/all_gather | solution.py:133
  260.7 393.2 %all-gather.18.cloned.1.call-start = ((), (), s32[]{:S(2)}) async-start(), calls=%async_computation.7 | async-start | bytes 17825792 | tf_op jit(solution)/shard_map/all_gather | solution.py:127
  261.4 415.2 %reduce-scatter.5.cloned.1.call-start = ((), (), s32[]{:S(2)}) async-start(), calls=%async_computation.8 | async-start | bytes 1179648 | tf_op jit(solution)/shard_map/reduce_scatter | solution.py:136
  653.9 22.7 %copy-start.7 = (bf16[96,2048]{1,0:T(8,128)(2,1)S(1)}, bf16[96,2048]{1,0:T(8,128)(2,1)}, u32[]{:S(2)}) copy-start(bf16[96,2048]{1,0:T(8,128)(2,1)} %reduce-scatter.3.cloned.1.call-done) | copy-start | bytes 1179652
  653.9 24.6 %copy-start.1 = (bf16[256,2048]{1,0:T(8,128)(2,1)S(1)}, bf16[256,2048]{1,0:T(8,128)(2,1)}, u32[]{:S(2)}) copy-start(bf16[256,2048]{1,0:T(8,128)(2,1)} %param.23) | copy-start | bytes 3145732
Sparse Core Ops, SparseCore 0:
  10.1 60.9 all-gather.9
  73.8 56.6 all-gather.13
  133.3 56.6 all-gather.11
  192.7 56.7 all-gather.15
  260.2 6.8 reduce-scatter.2
  269.8 192.1 all-gather.19
  464.7 189.1 all-gather.17
  670.3 6.3 reduce-scatter.4
